TPU v7x, 32 devices: a whole 2x2x4 slice. The times are simulated.
32 devices in a mesh: grp: 2 (over y), fs: 4 (over z), tp: 4 (over x, core).
Axes of the slice: x: 2, y: 2, z: 4, core: 2. Of those that a mesh axis runs over, the one named last changes fastest.
Arguments:
- tokens: bfloat16 [4096, 2048], P(('grp', 'fs'), 'tp'), parts along dimension 0, may hold values from -6 to 6
- first_gain: bfloat16 [2048], replicated, may hold values from 0.099609375 to 1.8984375
- u_proj: bfloat16 [2048, 1024], P('fs', 'tp'), may hold values from -0.125 to 0.125
- v_proj: bfloat16 [2048, 1024], P('fs', 'tp'), may hold values from -0.125 to 0.125
- group_gain: bfloat16 [8, 128], P('tp'), may hold values from 0.099609375 to 1.8984375
- spatial: bfloat16 [8, 128, 128], P('tp'), may hold values from -0.5 to 0.5
- spatial_bias: bfloat16 [8, 128], P('tp'), may hold values from 0.099609375 to 1.8984375
- mix_proj: bfloat16 [1024, 2048], P('fs', 'tp'), may hold values from -0.1875 to 0.1875
- second_gain: bfloat16 [2048], replicated, may hold values from 0.099609375 to 1.8984375
- up_proj: bfloat16 [2048, 8192], P('fs', 'tp'), may hold values from -0.125 to 0.125
- down_proj: bfloat16 [8192, 2048], P('tp', 'fs'), may hold values from -0.0625 to 0.0625
Outputs:
- layer_out: bfloat16 [4096, 2048], P(('grp', 'fs'), 'tp'), parts along dimension 0
There are 2 independent parts, one for each index of `grp`. A program takes and returns all parts, laid end to end along the dimension named above; an argument that names none is the same for every part. Nothing has to cross between parts.
All inputs are finite; a program needn't handle non-finite values.
Results may differ from a plain program's by a relative error of at most 0.017.
Values may be sent and summed in bfloat16 or wider, within the bound.
A program may use at most 64 MiB of HBM per device.

v0:
```python
import jax
import jax.numpy as jnp
from jax import lax
from jax.sharding import PartitionSpec as P

EPS = 1e-06


def rms_scale(values, gain_vec):
    mean_sq = jnp.mean(values * values, axis=-1, keepdims=True)
    return values * lax.rsqrt(mean_sq + EPS) * gain_vec.astype(jnp.float32)


def per_device(
    tokens,
    first_gain,
    u_proj,
    v_proj,
    group_gain,
    spatial,
    spatial_bias,
    mix_proj,
    second_gain,
    up_proj,
    down_proj,
):
    whole_rows = lax.all_gather(tokens, "tp", axis=1, tiled=True)
    row_count = whole_rows.shape[0]
    normed_rows = rms_scale(whole_rows.astype(jnp.float32), first_gain).astype(jnp.bfloat16)
    local_width = u_proj.shape[1]
    column_part = normed_rows
    u_pre = jnp.dot(
        column_part,
        lax.all_gather(u_proj, "fs", axis=0, tiled=True),
        preferred_element_type=jnp.float32,
    )
    v_pre = jnp.dot(
        column_part,
        lax.all_gather(v_proj, "fs", axis=0, tiled=True),
        preferred_element_type=jnp.float32,
    )
    u_act = jax.nn.gelu(u_pre).astype(jnp.bfloat16)
    local_groups = group_gain.shape[0]
    group_width = group_gain.shape[1]
    v_groups = jax.nn.gelu(v_pre).reshape(row_count, local_groups, group_width)
    v_normed = rms_scale(v_groups, group_gain).astype(jnp.bfloat16)
    block_len = spatial.shape[1]
    block_view = v_normed.reshape(row_count // block_len, block_len, local_groups, group_width)
    causal_mask = jnp.tril(jnp.ones((block_len, block_len), jnp.bool_))
    masked_weights = jnp.where(causal_mask[None], spatial, jnp.zeros_like(spatial))
    mixed_vals = jnp.einsum(
        "gts,nsgd->ntgd", masked_weights, block_view, preferred_element_type=jnp.float32
    )
    mixed_vals = mixed_vals + spatial_bias.astype(jnp.float32).T[None, :, :, None]
    gated_vals = (u_act.astype(jnp.float32) * mixed_vals.reshape(row_count, local_width)).astype(
        jnp.bfloat16
    )
    gated_whole = lax.all_gather(gated_vals, "tp", axis=1, tiled=True)
    column_part = gated_whole
    mix_vals = jnp.dot(
        column_part,
        lax.all_gather(mix_proj, "fs", axis=0, tiled=True),
        preferred_element_type=jnp.float32,
    )
    mid_stream = (tokens.astype(jnp.float32) + mix_vals).astype(jnp.bfloat16)
    mid_whole = lax.all_gather(mid_stream, "tp", axis=1, tiled=True)
    normed_two = rms_scale(mid_whole.astype(jnp.float32), second_gain).astype(jnp.bfloat16)
    column_part = normed_two
    pre_act = jnp.dot(
        column_part,
        lax.all_gather(up_proj, "fs", axis=0, tiled=True),
        preferred_element_type=jnp.float32,
    )
    hidden_act = jnp.square(jax.nn.relu(pre_act)).astype(jnp.bfloat16)
    down_terms = jnp.dot(
        hidden_act,
        lax.all_gather(down_proj, "fs", axis=1, tiled=True),
        preferred_element_type=jnp.float32,
    )
    down_sum = lax.psum_scatter(
        down_terms.astype(jnp.bfloat16), "tp", scatter_dimension=1, tiled=True
    ).astype(jnp.float32)
    return (mid_stream.astype(jnp.float32) + down_sum).astype(jnp.bfloat16)


def solution(mesh):
    return jax.shard_map(
        per_device,
        mesh=mesh,
        in_specs=(
            P(("grp", "fs"), "tp"),
            P(),
            P("fs", "tp"),
            P("fs", "tp"),
            P("tp", None),
            P("tp", None, None),
            P("tp", None),
            P("fs", "tp"),
            P(),
            P("fs", "tp"),
            P("tp", "fs"),
        ),
        out_specs=P(("grp", "fs"), "tp"),
        check_vma=False,
    )
```

profile of v0, /device:TPU:0, one launch (start us, length us, event | category | flops | bytes accessed | tf_op | source)
XLA Modules:
  0.0 520.2 jit_solution(6290348988835134259)
XLA Ops:
  6.5 0.7 all-gather.9.cloned.1.call-update
  7.3 0.7 all-gather.13.cloned.1.call-update
  8.1 0.7 all-gather.11.cloned.1.call-update
  8.8 0.5 all-gather.17.cloned.1.call-update
  9.4 0.7 convert_element_type.58
  10.1 0.7 convert_bitcast_fusion
  10.7 0.7 convert_element_type.62
  11.4 22.8 %all-gather.9.cloned.1.call-done = bf16[512,2048]{1,0:T(8,128)(2,1)} async-done(((bf16[512,512]{1,0:T(8,128)(2,1)}), bf16[512,2048]{1,0:T(8,128)(2,1)}) %all-gather.9.cloned.1.call-update) | async-done | bytes 2097168 | tf_op jit(solution)/shard_map/all_gather | solution.py:27
  34.2 2.1 fusion
  36.3 27.5 %all-gather.13.cloned.1.call-done = bf16[2048,256]{1,0:T(8,128)(2,1)} async-done(((bf16[512,256]{1,0:T(8,128)(2,1)}), bf16[2048,256]{1,0:T(8,128)(2,1)}) %all-gather.13.cloned.1.call-update) | async-done | bytes 1048592 | tf_op jit(solution)/shard_map/all_gather | solution.py:39
  63.8 3.5 fusion.52
  67.3 0.3 mul.103
  67.6 0.6 reduce_sum.28
  68.2 0.1 copy.24
  68.3 1.3 reshape.52
  69.7 0.2 copy.25
  69.9 0.3 fusion.10
  70.2 1.0 copy.26
  71.2 21.6 %all-gather.11.cloned.1.call-done = bf16[2048,256]{1,0:T(8,128)(2,1)} async-done(((bf16[512,256]{1,0:T(8,128)(2,1)}), bf16[2048,256]{1,0:T(8,128)(2,1)}) %all-gather.11.cloned.1.call-update) | async-done | bytes 1048592 | tf_op jit(solution)/shard_map/all_gather | solution.py:34
  92.8 2.9 fusion.33
  95.8 25.8 %all-gather.17.cloned.1.call-done = bf16[1024,512]{1,0:T(8,128)(2,1)} async-done(((bf16[256,512]{1,0:T(8,128)(2,1)}), bf16[1024,512]{1,0:T(8,128)(2,1)}) %all-gather.17.cloned.1.call-update) | async-done | bytes 1048592 | tf_op jit(solution)/shard_map/all_gather | solution.py:62
  121.6 17.6 %all-gather.15.cloned.1.call-done = bf16[512,1024]{1,0:T(8,128)(2,1)} async-done(((bf16[512,256]{1,0:T(8,128)(2,1)}), bf16[512,1024]{1,0:T(8,128)(2,1)}) %all-gather.15.cloned.1.call-update) | async-done | bytes 1048592 | tf_op jit(solution)/shard_map/all_gather | solution.py:58
  139.2 3.0 fusion.9
  142.3 0.7 all-gather.21.cloned.1.call-update
  143.1 0.7 all-gather.23.cloned.1.call-update
  143.9 21.1 %all-gather.19.cloned.1.call-done = bf16[512,2048]{1,0:T(8,128)(2,1)} async-done(((bf16[512,512]{1,0:T(8,128)(2,1)}), bf16[512,2048]{1,0:T(8,128)(2,1)}) %all-gather.19.cloned.1.call-update) | async-done | bytes 2097168 | tf_op jit(solution)/shard_map/all_gather | solution.py:66
  165.0 2.1 fusion.3
  167.1 149.1 %all-gather.21.cloned.1.call-done = bf16[2048,2048]{1,0:T(8,128)(2,1)} async-done(((bf16[512,2048]{1,0:T(8,128)(2,1)}), bf16[2048,2048]{1,0:T(8,128)(2,1)}) %all-gather.21.cloned.1.call-update) | async-done | bytes 8388624 | tf_op jit(solution)/shard_map/all_gather | solution.py:71
  316.2 149.4 %all-gather.23.cloned.1.call-done = bf16[2048,2048]{1,0:T(8,128)(2,1)} async-done(((bf16[2048,512]{1,0:T(8,128)(2,1)}), bf16[2048,2048]{1,0:T(8,128)(2,1)}) %all-gather.23.cloned.1.call-update) | async-done | bytes 8388624 | tf_op jit(solution)/shard_map/all_gather | solution.py:77
  465.6 16.6 %convolution_convert_fusion = bf16[512,2048]{1,0:T(8,128)(2,1)} fusion(bf16[2048,2048]{1,0:T(8,128)(2,1)} %all-gather.23.cloned.1.call-done, bf16[2048,2048]{1,0:T(8,128)(2,1)} %all-gather.21.cloned.1.call-done, bf16[512,2048]{1,0:T(8,128)(2,1)} %all-gather.19.cloned.1.call-done, f32[2048]{0:T(1024)S(1)} %convert_element_type.68, f32[512]{0:T(512)S(1)} %add_rsqrt_fusion.1), kind=kOutput, calls=%fused_computation.11 | convolution fusion | flops 8598323200 | bytes 20981760 | tf_op jit(solution)/shard_map/dot_general | solution.py:75
  482.2 29.5 %reduce-scatter.2.cloned.1.call-done = bf16[512,512]{1,0:T(8,128)(2,1)} async-done(((bf16[512,2048]{1,0:T(8,128)(2,1)}), bf16[512,512]{1,0:T(8,128)(2,1)}) %reduce-scatter.2.cloned.1.call-update) | async-done | bytes 524304 | tf_op jit(solution)/shard_map/reduce_scatter | solution.py:80
  511.7 2.0 add_convert_fusion
  (27 shorter events, 0.5 us)
Async XLA Ops:
  6.5 27.7 %all-gather.9.cloned.1.call-start = ((), (), s32[]{:S(2)}) async-start(), calls=%async_computation.1 | async-start | bytes 2621440 | tf_op jit(solution)/shard_map/all_gather | solution.py:27
  7.3 56.5 %all-gather.13.cloned.1.call-start = ((), (), s32[]{:S(2)}) async-start(), calls=%async_computation.3 | async-start | bytes 1310720 | tf_op jit(solution)/shard_map/all_gather | solution.py:39
  8.0 84.8 %all-gather.11.cloned.1.call-start = ((), (), s32[]{:S(2)}) async-start(), calls=%async_computation.2 | async-start | bytes 1310720 | tf_op jit(solution)/shard_map/all_gather | solution.py:34
  8.7 112.9 %all-gather.17.cloned.1.call-start = ((), (), s32[]{:S(2)}) async-start(), calls=%async_computation.5 | async-start | bytes 1310720 | tf_op jit(solution)/shard_map/all_gather | solution.py:62
  9.3 129.9 %all-gather.15.cloned.1.call-start = ((), (), s32[]{:S(2)}) async-start(), calls=%async_computation.4 | async-start | bytes 1310720 | tf_op jit(solution)/shard_map/all_gather | solution.py:58
  36.3 33.6 %copy-start.3 = (bf16[2,128,128]{2,1,0:T(8,128)(2,1)S(1)}, bf16[2,128,128]{2,1,0:T(8,128)(2,1)}, u32[]{:S(2)}) copy-start(bf16[2,128,128]{2,1,0:T(8,128)(2,1)} %param.16) | copy-start | bytes 196612
  67.3 25.5 %copy-start.1 = (bf16[512,2048]{1,0:T(8,128)(2,1)S(1)}, bf16[512,2048]{1,0:T(8,128)(2,1)}, u32[]{:S(2)}) copy-start(bf16[512,2048]{1,0:T(8,128)(2,1)} %all-gather.9.cloned.1.call-done) | copy-start | bytes 6291460
  70.2 69.1 %copy-start.2 = (bf16[512,512]{1,0:T(8,128)(2,1)S(1)}, bf16[512,512]{1,0:T(8,128)(2,1)}, u32[]{:S(2)}) copy-start(bf16[512,512]{1,0:T(8,128)(2,1)} %param.11) | copy-start | bytes 1572868
  95.7 48.1 %copy-start.4 = (bf16[2048]{0:T(1024)(128)(2,1)S(1)}, bf16[2048]{0:T(1024)(128)(2,1)}, u32[]{:S(2)}) copy-start(bf16[2048]{0:T(1024)(128)(2,1)} %param.19) | copy-start | bytes 12292
  95.7 69.3 %all-gather.19.cloned.1.call-start = ((), (), s32[]{:S(2)}) async-start(), calls=%async_computation.6 | async-start | bytes 2621440 | tf_op jit(solution)/shard_map/all_gather | solution.py:66
  142.3 173.9 %all-gather.21.cloned.1.call-start = ((), (), s32[]{:S(2)}) async-start(), calls=%async_computation.7 | async-start | bytes 10485760 | tf_op jit(solution)/shard_map/all_gather | solution.py:71
  143.0 322.6 %all-gather.23.cloned.1.call-start = ((), (), s32[]{:S(2)}) async-start(), calls=%async_computation.8 | async-start | bytes 10485760 | tf_op jit(solution)/shard_map/all_gather | solution.py:77
  143.8 367.9 %reduce-scatter.2.cloned.1.call-start = ((), (), s32[]{:S(2)}) async-start(), calls=%async_computation.9 | async-start | bytes 2621440 | tf_op jit(solution)/shard_map/reduce_scatter | solution.py:80
  167.1 344.6 %copy-start = (bf16[512,512]{1,0:T(8,128)(2,1)S(1)}, bf16[512,512]{1,0:T(8,128)(2,1)}, u32[]{:S(2)}) copy-start(bf16[512,512]{1,0:T(8,128)(2,1)} %fusion.9) | copy-start | bytes 1572868
Sparse Core Ops, SparseCore 0:
  8.9 25.2 all-gather.8
  35.8 27.9 all-gather.12
  65.4 27.3 all-gather.10
  94.2 27.3 all-gather.16
  123.0 16.1 all-gather.14
  142.4 22.5 all-gather.18
  166.6 149.6 all-gather.20
  317.8 147.7 all-gather.22
  482.3 29.3 reduce-scatter.1
where the time goes:
time: 521 us; the launch traced here: 520 us
  waiting for transfers between devices  469 us (90%)
  matrix products  26.3 us (5%)
  between operations  13.3 us (3%)
  other arithmetic  8.82 us (2%)
    all_gather x1, waiting for transfers between devices, per_device(): lax.all_gather(down_proj, 'fs', axis=1, tiled=True)  149 us
    all_gather x1, waiting for transfers between devices, per_device(): lax.all_gather(up_proj, 'fs', axis=0, tiled=True)  149 us
    reduce_scatter x1, waiting for transfers between devices, per_device(): lax.psum_scatter(down_terms.astype(jnp.bfloat16), 'tp', scatter_dimension...  29.5 us
    all_gather x1, waiting for transfers between devices, per_device(): lax.all_gather(v_proj, 'fs', axis=0, tiled=True)  27.5 us
    all_gather x1, waiting for transfers between devices, per_device(): lax.all_gather(mix_proj, 'fs', axis=0, tiled=True)  25.8 us
    all_gather x1, waiting for transfers between devices, per_device(): whole_rows = lax.all_gather(tokens, 'tp', axis=1, tiled=True)  22.8 us
    all_gather x1, waiting for transfers between devices, per_device(): lax.all_gather(u_proj, 'fs', axis=0, tiled=True)  21.6 us
    all_gather x1, waiting for transfers between devices, per_device(): mid_whole = lax.all_gather(mid_stream, 'tp', axis=1, tiled=True)  21.1 us
  transfers between devices with their start and end apart: 9, of which 9 were waited for; matrix products, arithmetic and copies ran while one was open for 3% of the time, Pallas kernels for 0%

commit v1 on v0

--- a/solution.py
+++ b/solution.py
@@ -1,6 +1,10 @@
+import functools
+
 import jax
 import jax.numpy as jnp
 from jax import lax
+from jax.experimental import pallas as pl
+from jax.experimental.pallas import tpu as pltpu
 from jax.sharding import PartitionSpec as P
 
 EPS = 1e-06
@@ -83,9 +87,453 @@
     return (mid_stream.astype(jnp.float32) + down_sum).astype(jnp.bfloat16)
 
 
+def remote(src, dst, send, recv, where):
+    return pltpu.make_async_remote_copy(
+        src_ref=src,
+        dst_ref=dst,
+        send_sem=send,
+        recv_sem=recv,
+        device_id=where,
+        device_id_type=pl.DeviceIdType.MESH,
+    )
+
+
+def fused_kernel(
+    tok, gain1, u_w, v_w, ggain, spat, bias, mix_w, gain2, up_w, down_w,
+    out,
+    xg, uvg, mg, upg, dng, norm, gat, mid, hid, c_out, c_in, z_out, z_in, x_out, x_in,
+    z_send, z_recv, y_send, y_recv, l_sem, a_send, a_recv, c_send, c_recv, r_send, r_recv,
+    s_send, s_recv,
+):
+    y, z, t = lax.axis_index("grp"), lax.axis_index("fs"), lax.axis_index("tp")
+    q, c, x = lax.rem(z, 2), lax.rem(t, 2), t // 2
+    z_pair = z + 1 - 2 * q
+    t_core, t_chip = t + 1 - 2 * c, lax.rem(t + 2, 4)
+    to_y, to_z = (1 - y, z, t), (y, z_pair, t)
+    to_c, to_x = (y, z, t_core), (y, z, t_chip)
+    others = (lax.rem(z + 2, 4), 3 - z, z_pair)
+    rows, width = tok.shape
+    all_rows = 2 * rows
+    step = 256
+    f32, bf16 = jnp.float32, jnp.bfloat16
+
+    barrier = pltpu.get_barrier_semaphore()
+    for where in (to_y, to_c, to_x) + tuple((y, o, t) for o in others):
+        pl.semaphore_signal(
+            barrier, inc=1, device_id=where, device_id_type=pl.DeviceIdType.MESH
+        )
+    pl.semaphore_wait(barrier, 6)
+
+    gw = ggain.shape[1]
+    ur, mr, mc = u_w.shape[0], mix_w.shape[0], mix_w.shape[1] // 2
+    pr, pc = up_w.shape[0], up_w.shape[1] // 2
+    dr = down_w.shape[0] // 2
+
+    def half(size, which):
+        return pl.ds(pl.multiple_of(which * size, size), size)
+
+    def take(w, par, which):
+        if w == 0:
+            return u_w.at[slice(None) if which is None else half(ur // 2, which), half(gw, par)]
+        if w == 1:
+            return v_w.at[slice(None) if which is None else half(ur // 2, which), half(gw, par)]
+        if w == 2:
+            return mix_w.at[slice(None) if which is None else half(mr // 2, which), half(mc, par)]
+        if w == 3:
+            return up_w.at[slice(None) if which is None else half(pr // 2, which), half(pc, par)]
+        if which is None:
+            return down_w.at[half(dr, par), :]
+        return down_w.at[half(dr // 2, 2 * par + which), :]
+
+    def put(w, source, which):
+        if w < 2:
+            cols = pl.ds(w * gw, gw)
+            if which is None:
+                return uvg.at[half(ur, source), cols]
+            return uvg.at[half(ur // 2, 2 * source + which), cols]
+        if w == 2:
+            return mg.at[half(mr, source) if which is None else half(mr // 2, 2 * source + which), :]
+        if w == 3:
+            return upg.at[half(pr, source) if which is None else half(pr // 2, 2 * source + which), :]
+        if which is None:
+            return dng.at[source]
+        return dng.at[source, half(dr // 2, which), :]
+
+    def z_copy(w, dest):
+        return remote(
+            take(w, lax.rem(dest, 2), y), put(w, z, y), z_send.at[w, dest], z_recv.at[w, z],
+            (y, dest, t),
+        )
+
+    def z_arrived(w, source):
+        return remote(
+            put(w, source, y), put(w, source, y), z_send.at[w, source], z_recv.at[w, source],
+            (y, source, t),
+        )
+
+    def y_copy(w, source):
+        return remote(
+            put(w, source, y), put(w, source, y), y_send.at[w, source], y_recv.at[w, source], to_y
+        )
+
+    def y_arrived(w, source):
+        return remote(
+            put(w, source, 1 - y), put(w, source, 1 - y), y_send.at[w, source],
+            y_recv.at[w, source], to_y,
+        )
+
+    def forward(w, source):
+        z_arrived(w, source).wait_recv()
+        y_copy(w, source).start()
+
+    def own_copy(w):
+        return pltpu.make_async_copy(take(w, q, None), put(w, z, None), l_sem.at[w])
+
+    def gather_copy(buf, a, n):
+        p, s, where = (
+            (q, t, to_z), (q, t, to_x), (q, t, to_c), (1 - q, t, to_x), (1 - q, t, to_c),
+            (q, t_chip, to_c), (1 - q, t_chip, to_c),
+        )[n]
+        return remote(
+            buf.at[p, s], buf.at[p, s], a_send.at[a, n], a_recv.at[a, n], where
+        )
+
+    def gather_arrived(buf, a, n):
+        p, s, where = (
+            (1 - q, t, to_z), (q, t_chip, to_x), (q, t_core, to_c), (1 - q, t_chip, to_x),
+            (1 - q, t_core, to_c), (q, 3 - t, to_c), (1 - q, 3 - t, to_c),
+        )[n]
+        return remote(
+            buf.at[p, s], buf.at[p, s], a_send.at[a, n], a_recv.at[a, n], where
+        )
+
+    def gather_start(buf, a):
+        for n in (0, 1, 2):
+            gather_copy(buf, a, n).start()
+
+    def gather_finish(buf, a):
+        gather_arrived(buf, a, 0).wait_recv()
+        gather_copy(buf, a, 3).start()
+        gather_copy(buf, a, 4).start()
+        gather_arrived(buf, a, 1).wait_recv()
+        gather_copy(buf, a, 5).start()
+        gather_arrived(buf, a, 3).wait_recv()
+        gather_copy(buf, a, 6).start()
+        for n in (2, 4, 5, 6):
+            gather_arrived(buf, a, n).wait_recv()
+
+    own_tok = pltpu.make_async_copy(tok, xg.at[q, t], l_sem.at[5])
+    own_tok.start()
+    own_tok.wait()
+    gather_start(xg, 0)
+    for w in range(5):
+        own_copy(w).start()
+    for w in range(3):
+        for o in others:
+            z_copy(w, o).start()
+    for o in others[:2]:
+        z_copy(3, o).start()
+
+    gather_finish(xg, 0)
+    for w in range(3):
+        for o in others:
+            forward(w, o)
+
+    def scaled(pieces, gain):
+        total = pieces[0].shape[0]
+        sums = jnp.zeros((total, 1), f32)
+        for piece in pieces:
+            sums += jnp.sum(piece * piece, axis=-1, keepdims=True)
+        count = sum(piece.shape[1] for piece in pieces)
+        scale = lax.rsqrt(sums / count + EPS)
+        at = 0
+        res = []
+        for piece in pieces:
+            wide = piece.shape[1]
+            res.append((piece * scale * gain[:, at : at + wide]).astype(bf16))
+            at += wide
+        return jnp.concatenate(res, axis=1)
+
+    small = 64
+    per_part = rows // small
+    gain_one = gain1[...].astype(f32)
+    gain_two = gain2[...].astype(f32)
+
+    def norm_one(i, carry):
+        p, r = i // per_part, pl.multiple_of(lax.rem(i, per_part) * small, small)
+        pieces = [xg[p, s, pl.ds(r, small), :].astype(f32) for s in range(4)]
+        norm[pl.ds(pl.multiple_of(i * small, small), small), :] = scaled(pieces, gain_one)
+        return carry
+
+    lax.fori_loop(0, all_rows // small, norm_one, 0)
+
+    for w in range(2):
+        own_copy(w).wait()
+        for o in others:
+            y_arrived(w, o).wait_recv()
+
+    blk = spat.shape[1]
+    lower = lax.broadcasted_iota(jnp.int32, (blk, blk), 0) >= lax.broadcasted_iota(
+        jnp.int32, (blk, blk), 1
+    )
+    mixer = jnp.where(lower, spat[q].astype(f32), 0.0).astype(bf16)
+    shift = jnp.where(q == 0, bias[:, 0:1], bias[:, 1:2])
+    gain_g = jnp.where(q == 0, ggain[0:1, :], ggain[1:2, :])
+
+    def mix_rows(i, carry):
+        here = pl.ds(pl.multiple_of(i * step, step), step)
+        both = jnp.dot(norm[here, :], uvg[...], preferred_element_type=f32)
+        both = jax.nn.gelu(both)
+        u_act = both[:, :gw].astype(bf16).astype(f32)
+        v_act = both[:, gw:]
+        v_n = (
+            v_act
+            * lax.rsqrt(jnp.mean(v_act * v_act, axis=-1, keepdims=True) + EPS)
+            * gain_g
+        ).astype(bf16)
+        for b in range(step // blk):
+            part = slice(b * blk, (b + 1) * blk)
+            mixed = jnp.dot(mixer, v_n[part], preferred_element_type=f32) + shift
+            gat[q, t, pl.ds(pl.multiple_of(i * step + b * blk, blk), blk), :] = (
+                u_act[part] * mixed
+            ).astype(bf16)
+        return carry
+
+    lax.fori_loop(0, all_rows // step, mix_rows, 0)
+    gather_start(gat, 1)
+    z_copy(3, others[2]).start()
+    for o in others[:2]:
+        z_copy(4, o).start()
+    gather_finish(gat, 1)
+    own_copy(2).wait()
+    for o in others:
+        y_arrived(2, o).wait_recv()
+
+    def middle_rows(i, carry):
+        here = pl.ds(pl.multiple_of(i * step, step), step)
+        p = i // (rows // step)
+        within = pl.ds(pl.multiple_of(lax.rem(i, rows // step) * step, step), step)
+        left = jnp.concatenate([gat[k % 2, k // 2, here, :] for k in range(8)], axis=1)
+        value = jnp.dot(left, mg[...], preferred_element_type=f32)
+        value += xg[p, t, within, half(mc, q)].astype(f32)
+        mid[q, t, here, :] = value.astype(bf16)
+        return carry
+
+    lax.fori_loop(0, all_rows // step, middle_rows, 0)
+    gather_start(mid, 2)
+    z_copy(4, others[2]).start()
+    for o in others[:2]:
+        forward(3, o)
+    gather_finish(mid, 2)
+    forward(3, others[2])
+
+    def norm_two(i, carry):
+        here = pl.ds(pl.multiple_of(i * small, small), small)
+        pieces = [mid[k % 2, k // 2, here, :].astype(f32) for k in range(8)]
+        norm[here, :] = scaled(pieces, gain_two)
+        return carry
+
+    lax.fori_loop(0, all_rows // small, norm_two, 0)
+    own_copy(3).wait()
+    for o in others:
+        y_arrived(3, o).wait_recv()
+
+    def up_rows(i, carry):
+        here = pl.ds(pl.multiple_of(i * step, step), step)
+        pre = jnp.dot(norm[here, :], upg[...], preferred_element_type=f32)
+        hid[here, :] = jnp.square(jax.nn.relu(pre)).astype(bf16)
+        return carry
+
+    lax.fori_loop(0, all_rows // step, up_rows, 0)
+
+    near, far = z // 2, 1 - z // 2
+    order = (2 * near + 1 - c, 2 * near + c, 2 * far + 1 - c, 2 * far + c)
+
+    def fetch(quarter):
+        @pl.when(quarter != z)
+        def _():
+            forward(4, quarter)
+
+    def ready(quarter):
+        @pl.when(quarter == z)
+        def _():
+            own_copy(4).wait()
+
+        @pl.when(quarter != z)
+        def _():
+            y_arrived(4, quarter).wait_recv()
+
+    def down_part(quarter, start):
+        return jnp.dot(
+            hid[pl.ds(start, step), :], dng[quarter], preferred_element_type=f32
+        )
+
+    def core_copy(n):
+        return remote(c_out.at[n], c_in.at[n], c_send.at[n], c_recv.at[n], to_c)
+
+    def pair_copy(n):
+        return remote(z_out.at[n], z_in.at[n], r_send.at[n], r_recv.at[n], to_z)
+
+    def chip_copy():
+        return remote(x_out, x_in, s_send.at[0], s_recv.at[0], to_x)
+
+    def give(n):
+        quarter = order[2 * n]
+        ready(quarter)
+
+        def loop(i, carry):
+            start = pl.multiple_of(i * step, step)
+            c_out[n, pl.ds(start, step), :] = down_part(quarter, start).astype(bf16)
+            return carry
+
+        lax.fori_loop(0, all_rows // step, loop, 0)
+        core_copy(n).start()
+
+    def keep(n):
+        quarter = order[2 * n + 1]
+        ready(quarter)
+        core_copy(n).wait_recv()
+
+        def loop_other(i, carry):
+            off = pl.multiple_of(i * step, step)
+            start = pl.multiple_of((1 - q) * rows + i * step, step)
+            value = down_part(quarter, start) + c_in[n, pl.ds(start, step), :].astype(f32)
+            z_out[n, pl.ds(off, step), :] = value.astype(bf16)
+            return carry
+
+        lax.fori_loop(0, rows // step, loop_other, 0)
+        pair_copy(n).start()
+
+        def loop_own(i, carry):
+            off = pl.multiple_of(i * step, step)
+            start = pl.multiple_of(q * rows + i * step, step)
+            value = down_part(quarter, start) + c_in[n, pl.ds(start, step), :].astype(f32)
+            c_in[n, pl.ds(start, step), :] = value.astype(bf16)
+            return carry
+
+        lax.fori_loop(0, rows // step, loop_own, 0)
+
+    fetch(order[0])
+    fetch(order[1])
+    give(0)
+    fetch(order[2])
+    keep(0)
+    fetch(order[3])
+    give(1)
+    keep(1)
+
+    mine = pl.ds(pl.multiple_of(q * rows, rows), rows)
+
+    def total(n, i):
+        off = pl.multiple_of(i * step, step)
+        start = pl.multiple_of(q * rows + i * step, step)
+        return c_in[n, pl.ds(start, step), :].astype(f32) + z_in[n, pl.ds(off, step), :].astype(f32)
+
+    far_slot = jnp.where(near == x, 1, 0)
+    own_slot = 1 - far_slot
+
+    def send_far(i, carry):
+        x_out[pl.ds(pl.multiple_of(i * step, step), step), :] = total(far_slot, i).astype(bf16)
+        return carry
+
+    def finish(i, carry):
+        off = pl.multiple_of(i * step, step)
+        here = pl.ds(pl.multiple_of(q * rows + i * step, step), step)
+        value = total(own_slot, i) + x_in[pl.ds(off, step), :].astype(f32)
+        stream = jnp.concatenate([mid[0, t, here, :], mid[1, t, here, :]], axis=1)
+        out[pl.ds(off, step), :] = (value + stream.astype(f32)).astype(bf16)
+        return carry
+
+    pair_copy(0).wait_recv()
+
+    @pl.when(far_slot == 0)
+    def _():
+        lax.fori_loop(0, rows // step, send_far, 0)
+        chip_copy().start()
+
+    pair_copy(1).wait_recv()
+
+    @pl.when(far_slot == 1)
+    def _():
+        lax.fori_loop(0, rows // step, send_far, 0)
+        chip_copy().start()
+
+    chip_copy().wait_recv()
+    lax.fori_loop(0, rows // step, finish, 0)
+
+    for w in range(5):
+        for o in others:
+            z_copy(w, o).wait_send()
+            y_copy(w, o).wait_send()
+    for a, buf in enumerate((xg, gat, mid)):
+        for n in range(7):
+            gather_copy(buf, a, n).wait_send()
+    for n in range(2):
+        core_copy(n).wait_send()
+        pair_copy(n).wait_send()
+    chip_copy().wait_send()
+
+
+def fused(tokens, first_gain, u_proj, v_proj, group_gain, spatial, spatial_bias, mix_proj,
+          second_gain, up_proj, down_proj):
+    rows, width = tokens.shape
+    both, wide, gw = 2 * rows, second_gain.shape[0], group_gain.shape[1]
+    vmem, bf16, dma = pltpu.VMEM, jnp.bfloat16, pltpu.SemaphoreType.DMA
+    spec = pl.BlockSpec(memory_space=pltpu.VMEM)
+    ff = up_proj.shape[1] // 2
+    return pl.pallas_call(
+        fused_kernel,
+        out_shape=jax.ShapeDtypeStruct(tokens.shape, tokens.dtype),
+        in_specs=[spec] * 11,
+        out_specs=spec,
+        scratch_shapes=[
+            vmem((2, 4, rows, width), bf16),
+            vmem((wide, 2 * gw), bf16),
+            vmem((4 * mix_proj.shape[0], width // 2), bf16),
+            vmem((wide, ff), bf16),
+            vmem((4, ff, down_proj.shape[1]), bf16),
+            vmem((both, wide), bf16),
+            vmem((2, 4, both, gw), bf16),
+            vmem((2, 4, both, width // 2), bf16),
+            vmem((both, ff), bf16),
+            vmem((2, both, width), bf16),
+            vmem((2, both, width), bf16),
+            vmem((2, rows, width), bf16),
+            vmem((2, rows, width), bf16),
+            vmem((rows, width), bf16),
+            vmem((rows, width), bf16),
+            dma((5, 4)), dma((5, 4)), dma((5, 4)), dma((5, 4)), dma((6,)),
+            dma((3, 7)), dma((3, 7)), dma((2,)), dma((2,)), dma((2,)), dma((2,)),
+            dma((1,)), dma((1,)),
+        ],
+        compiler_params=pltpu.CompilerParams(
+            collective_id=0, has_side_effects=True, vmem_limit_bytes=64 * 1024 * 1000
+        ),
+    )(
+        tokens, first_gain[None], u_proj, v_proj, group_gain.astype(jnp.float32), spatial,
+        spatial_bias.astype(jnp.float32).T, mix_proj, second_gain[None], up_proj, down_proj,
+    )
+
+
+def layer_part(axes, *args):
+    tokens, group_gain, spatial = args[0], args[4], args[5]
+    fits = (
+        axes["grp"] == 2
+        and axes["fs"] == 4
+        and axes["tp"] == 4
+        and group_gain.shape[0] == 2
+        and group_gain.shape[1] % 128 == 0
+        and tokens.shape[0] % 256 == 0
+        and tokens.shape[1] % 256 == 0
+        and tokens.shape[1] == args[10].shape[1]
+        and 256 % spatial.shape[1] == 0
+    )
+    return fused(*args) if fits else per_device(*args)
+
+
 def solution(mesh):
     return jax.shard_map(
-        per_device,
+        functools.partial(layer_part, dict(mesh.shape)),
         mesh=mesh,
         in_specs=(
             P(("grp", "fs"), "tp"),

time: 521 us -> 214 us (0.41)
  waiting for transfers between devices: 469 us -> 0 us
  Pallas kernels: 0 us -> 206 us
  matrix products: 26.3 us -> 0 us
  between operations: 13.3 us -> 0.01 us
  other arithmetic: 8.82 us -> 1.23 us
    all_gather x8 -> x0, waiting for transfers between devices: 435 us -> none  [the longest x1 149 us: per_device(): lax.all_gather(down_proj, 'fs', axis=1, tiled=True)]
    pallas_call x0 -> x1, Pallas kernels: none -> 206 us  [fused(): pl.pallas_call(fused_kernel, out_shape=jax.ShapeDtypeStruct(tokens.shape,...]
    reduce_scatter x1 -> x0, waiting for transfers between devices: 29.5 us -> none  [per_device(): lax.psum_scatter(down_terms.astype(jnp.bfloat16), 'tp', scatter_dimension...]
    dot_general x5 -> x0, matrix products: 26.3 us -> none  [the longest x1 16.6 us: per_device(): jnp.dot(hidden_act, lax.all_gather(down_proj, 'fs', axis=1, tiled=True),...]
  transfers between devices with their start and end apart: 9 -> 0, of which waited for: 9 -> 0; matrix products, arithmetic and copies ran while one was open for 3% -> 0% of each run, Pallas kernels for 0% -> 0%
where the time goes in v1:
time: 214 us
  Pallas kernels  206 us (96%)
  local copies, waits for them, and re-layouts  5.83 us (3%)
    pallas_call x1, Pallas kernels, fused(): pl.pallas_call(fused_kernel, out_shape=jax.ShapeDtypeStruct(tokens.shape,...  206 us

profile of v1, /device:TPU:0, one launch (start us, length us, event | category | flops | bytes accessed | tf_op | source)
XLA Modules:
  0.0 213.5 jit_solution(13855410466022592807)
XLA Ops:
  0.0 1.2 convert_element_type.4.ggain
  1.2 1.3 broadcast_in_dim.6.gain1
  2.5 1.3 broadcast_in_dim.7.gain2
  3.8 1.4 copy.12
  5.2 206.4 %shard_map.109 = bf16[512,512]{1,0:T(8,128)(2,1)} custom-call(bf16[512,512]{1,0:T(8,128)(2,1)} %tok.1, bf16[1,2048]{1,0:T(2,128)(2,1)} %broadcast_in_dim.6.gain1, bf16[512,256]{1,0:T(8,128)(2,1)} %u_w.1, bf16[512,256]{1,0:T(8,128)(2,1)} %v_w.1, f32[2,128]{1,0:T(2,128)} %convert_element_type.4.ggain, bf16[2,128,128]{2,1,0:T(8,128)(2,1)} %spat.1, ...), custom_call_target="tpu_custom_call" | custom-call | tf_op jit(solution)/shard_map/pallas_call | solution.py:484
  211.7 1.9 copy.14

commit v2 on v1

v2 whole, which is shorter than its diff:
```python
import functools

import jax
import jax.numpy as jnp
from jax import lax
from jax.experimental import pallas as pl
from jax.experimental.pallas import tpu as pltpu
from jax.sharding import PartitionSpec as P

EPS = 1e-06


def rms_scale(values, gain_vec):
    mean_sq = jnp.mean(values * values, axis=-1, keepdims=True)
    return values * lax.rsqrt(mean_sq + EPS) * gain_vec.astype(jnp.float32)


def per_device(
    tokens,
    first_gain,
    u_proj,
    v_proj,
    group_gain,
    spatial,
    spatial_bias,
    mix_proj,
    second_gain,
    up_proj,
    down_proj,
):
    whole_rows = lax.all_gather(tokens, "tp", axis=1, tiled=True)
    row_count = whole_rows.shape[0]
    normed_rows = rms_scale(whole_rows.astype(jnp.float32), first_gain).astype(jnp.bfloat16)
    local_width = u_proj.shape[1]
    column_part = normed_rows
    u_pre = jnp.dot(
        column_part,
        lax.all_gather(u_proj, "fs", axis=0, tiled=True),
        preferred_element_type=jnp.float32,
    )
    v_pre = jnp.dot(
        column_part,
        lax.all_gather(v_proj, "fs", axis=0, tiled=True),
        preferred_element_type=jnp.float32,
    )
    u_act = jax.nn.gelu(u_pre).astype(jnp.bfloat16)
    local_groups = group_gain.shape[0]
    group_width = group_gain.shape[1]
    v_groups = jax.nn.gelu(v_pre).reshape(row_count, local_groups, group_width)
    v_normed = rms_scale(v_groups, group_gain).astype(jnp.bfloat16)
    block_len = spatial.shape[1]
    block_view = v_normed.reshape(row_count // block_len, block_len, local_groups, group_width)
    causal_mask = jnp.tril(jnp.ones((block_len, block_len), jnp.bool_))
    masked_weights = jnp.where(causal_mask[None], spatial, jnp.zeros_like(spatial))
    mixed_vals = jnp.einsum(
        "gts,nsgd->ntgd", masked_weights, block_view, preferred_element_type=jnp.float32
    )
    mixed_vals = mixed_vals + spatial_bias.astype(jnp.float32).T[None, :, :, None]
    gated_vals = (u_act.astype(jnp.float32) * mixed_vals.reshape(row_count, local_width)).astype(
        jnp.bfloat16
    )
    gated_whole = lax.all_gather(gated_vals, "tp", axis=1, tiled=True)
    column_part = gated_whole
    mix_vals = jnp.dot(
        column_part,
        lax.all_gather(mix_proj, "fs", axis=0, tiled=True),
        preferred_element_type=jnp.float32,
    )
    mid_stream = (tokens.astype(jnp.float32) + mix_vals).astype(jnp.bfloat16)
    mid_whole = lax.all_gather(mid_stream, "tp", axis=1, tiled=True)
    normed_two = rms_scale(mid_whole.astype(jnp.float32), second_gain).astype(jnp.bfloat16)
    column_part = normed_two
    pre_act = jnp.dot(
        column_part,
        lax.all_gather(up_proj, "fs", axis=0, tiled=True),
        preferred_element_type=jnp.float32,
    )
    hidden_act = jnp.square(jax.nn.relu(pre_act)).astype(jnp.bfloat16)
    down_terms = jnp.dot(
        hidden_act,
        lax.all_gather(down_proj, "fs", axis=1, tiled=True),
        preferred_element_type=jnp.float32,
    )
    down_sum = lax.psum_scatter(
        down_terms.astype(jnp.bfloat16), "tp", scatter_dimension=1, tiled=True
    ).astype(jnp.float32)
    return (mid_stream.astype(jnp.float32) + down_sum).astype(jnp.bfloat16)


def remote(src, dst, send, recv, where):
    return pltpu.make_async_remote_copy(
        src_ref=src,
        dst_ref=dst,
        send_sem=send,
        recv_sem=recv,
        device_id=where,
        device_id_type=pl.DeviceIdType.MESH,
    )


def fused_kernel(
    row_step,
    tok, gain1, u_w, v_w, ggain, spat, bias, mix_w, gain2, up_w, down_w,
    out,
    xg, uvg, mg, upg, dng, norm, gat, mid, hid, c_out, c_in, z_out, z_in, x_out, x_in,
    z_send, z_recv, y_send, y_recv, l_sem, a_send, a_recv, c_send, c_recv, r_send, r_recv,
    s_send, s_recv,
):
    y, z, t = lax.axis_index("grp"), lax.axis_index("fs"), lax.axis_index("tp")
    q, c, x = lax.rem(z, 2), lax.rem(t, 2), t // 2
    z_pair = z + 1 - 2 * q
    t_core, t_chip = t + 1 - 2 * c, lax.rem(t + 2, 4)
    to_y, to_z = (1 - y, z, t), (y, z_pair, t)
    to_c, to_x = (y, z, t_core), (y, z, t_chip)
    others = (lax.rem(z + 2, 4), 3 - z, z_pair)
    rows, width = tok.shape
    step = row_step
    f32, bf16 = jnp.float32, jnp.bfloat16

    barrier = pltpu.get_barrier_semaphore()
    for where in (to_y, to_c, to_x) + tuple((y, o, t) for o in others):
        pl.semaphore_signal(
            barrier, inc=1, device_id=where, device_id_type=pl.DeviceIdType.MESH
        )
    pl.semaphore_wait(barrier, 6)

    gw = ggain.shape[1]
    ur, mr, mc = u_w.shape[0], mix_w.shape[0], mix_w.shape[1] // 2
    pr, pc = up_w.shape[0], up_w.shape[1] // 2
    dr = down_w.shape[0] // 2

    def half(size, which):
        return pl.ds(pl.multiple_of(which * size, size), size)

    def take(w, par, which):
        if w == 0:
            return u_w.at[slice(None) if which is None else half(ur // 2, which), half(gw, par)]
        if w == 1:
            return v_w.at[slice(None) if which is None else half(ur // 2, which), half(gw, par)]
        if w == 2:
            return mix_w.at[slice(None) if which is None else half(mr // 2, which), half(mc, par)]
        if w == 3:
            return up_w.at[slice(None) if which is None else half(pr // 2, which), half(pc, par)]
        if which is None:
            return down_w.at[half(dr, par), :]
        return down_w.at[half(dr // 2, 2 * par + which), :]

    def put(w, source, which):
        if w < 2:
            cols = pl.ds(w * gw, gw)
            if which is None:
                return uvg.at[half(ur, source), cols]
            return uvg.at[half(ur // 2, 2 * source + which), cols]
        if w == 2:
            return mg.at[half(mr, source) if which is None else half(mr // 2, 2 * source + which), :]
        if w == 3:
            return upg.at[half(pr, source) if which is None else half(pr // 2, 2 * source + which), :]
        if which is None:
            return dng.at[source]
        return dng.at[source, half(dr // 2, which), :]

    def z_copy(w, dest):
        return remote(
            take(w, lax.rem(dest, 2), y), put(w, z, y), z_send.at[w, dest], z_recv.at[w, z],
            (y, dest, t),
        )

    def z_arrived(w, source):
        return remote(
            put(w, source, y), put(w, source, y), z_send.at[w, source], z_recv.at[w, source],
            (y, source, t),
        )

    def y_copy(w, source):
        return remote(
            put(w, source, y), put(w, source, y), y_send.at[w, source], y_recv.at[w, source], to_y
        )

    def y_arrived(w, source):
        return remote(
            put(w, source, 1 - y), put(w, source, 1 - y), y_send.at[w, source],
            y_recv.at[w, source], to_y,
        )

    def forward(w, source):
        z_arrived(w, source).wait_recv()
        y_copy(w, source).start()

    def own_copy(w):
        return pltpu.make_async_copy(take(w, q, None), put(w, z, None), l_sem.at[w])

    def gather_copy(a, h, n):
        p, s, where = (
            (q, t, to_z), (q, t, to_x), (q, t, to_c), (1 - q, t, to_x), (1 - q, t, to_c),
            (q, t_chip, to_c), (1 - q, t_chip, to_c),
        )[n]
        ref = piece(a, h, p, s)
        return remote(ref, ref, a_send.at[a, h, n], a_recv.at[a, h, n], where)

    def gather_arrived(a, h, n):
        p, s, where = (
            (1 - q, t, to_z), (q, t_chip, to_x), (q, t_core, to_c), (1 - q, t_chip, to_x),
            (1 - q, t_core, to_c), (q, 3 - t, to_c), (1 - q, 3 - t, to_c),
        )[n]
        ref = piece(a, h, p, s)
        return remote(ref, ref, a_send.at[a, h, n], a_recv.at[a, h, n], where)

    def piece(a, h, p, s):
        if a == 0:
            return xg.at[p, s, pl.ds(h * step, step), :]
        return (gat, mid)[a - 1].at[p, s, h]

    def gather_start(a, h):
        for n in (0, 1, 2):
            gather_copy(a, h, n).start()

    def gather_pair(a, h):
        gather_arrived(a, h, 0).wait_recv()
        gather_copy(a, h, 3).start()
        gather_copy(a, h, 4).start()

    def gather_rest(a, h):
        gather_arrived(a, h, 1).wait_recv()
        gather_copy(a, h, 5).start()
        gather_arrived(a, h, 3).wait_recv()
        gather_copy(a, h, 6).start()
        for n in (2, 4, 5, 6):
            gather_arrived(a, h, n).wait_recv()

    chunks = rows // step
    inner = (z + 1) // 2 == 1
    across, facing, pair = others

    own_tok = pltpu.make_async_copy(tok, xg.at[q, t], l_sem.at[5])
    own_tok.start()
    for w in range(2):
        for o in others:
            z_copy(w, o).start()
    own_tok.wait()
    for h in range(chunks):
        gather_start(0, h)
    for w in range(5):
        own_copy(w).start()

    @pl.when(inner)
    def _():
        z_copy(2, facing).start()
        z_copy(3, facing).start()

    for h in range(chunks):
        gather_pair(0, h)

    @pl.when(jnp.logical_not(inner))
    def _():
        z_copy(2, facing).start()

    for o in (across, pair):
        z_copy(2, o).start()
    z_copy(3, across).start()
    for w in range(2):
        for o in others:
            forward(w, o)

    def scaled(pieces, gain):
        total = pieces[0].shape[0]
        sums = jnp.zeros((total, 1), f32)
        for piece in pieces:
            sums += jnp.sum(piece * piece, axis=-1, keepdims=True)
        count = sum(piece.shape[1] for piece in pieces)
        scale = lax.rsqrt(sums / count + EPS)
        at = 0
        res = []
        for piece in pieces:
            wide = piece.shape[1]
            res.append((piece * scale * gain[:, at : at + wide]).astype(bf16))
            at += wide
        return jnp.concatenate(res, axis=1)

    small = 64
    per_part = step // small
    gain_one = gain1[...].astype(f32).reshape(1, -1)
    gain_two = gain2[...].astype(f32).reshape(1, -1)

    def norm_one(h):
        def loop(i, carry):
            p, r = i // per_part, pl.multiple_of(lax.rem(i, per_part) * small, small)
            pieces = [xg[p, s, pl.ds(h * step + r, small), :].astype(f32) for s in range(4)]
            at = pl.multiple_of(h * 2 * step + i * small, small)
            norm[pl.ds(at, small), :] = scaled(pieces, gain_one)
            return carry

        lax.fori_loop(0, 2 * per_part, loop, 0)

    blk = spat.shape[1]
    lower = lax.broadcasted_iota(jnp.int32, (blk, blk), 0) >= lax.broadcasted_iota(
        jnp.int32, (blk, blk), 1
    )
    mixer = jnp.where(lower, spat[q].astype(f32), 0.0).astype(bf16)
    eye = lax.broadcasted_iota(jnp.int32, (blk, blk), 0) == lax.broadcasted_iota(
        jnp.int32, (blk, blk), 1
    )
    bias_row = jnp.where(q == 0, bias[0:1, :].astype(f32), bias[1:2, :].astype(f32))
    shift = jnp.sum(jnp.where(eye, bias_row, 0.0), axis=1, keepdims=True)
    gain_g = jnp.where(q == 0, ggain[0:1, :].astype(f32), ggain[1:2, :].astype(f32))

    def mix_rows(h):
        def loop(i, carry):
            here = pl.ds(pl.multiple_of((2 * h + i) * step, step), step)
            both = jnp.dot(norm[here, :], uvg[...], preferred_element_type=f32)
            both = jax.nn.gelu(both)
            u_act = both[:, :gw].astype(bf16).astype(f32)
            v_act = both[:, gw:]
            v_n = (
                v_act
                * lax.rsqrt(jnp.mean(v_act * v_act, axis=-1, keepdims=True) + EPS)
                * gain_g
            ).astype(bf16)
            for b in range(step // blk):
                part = slice(b * blk, (b + 1) * blk)
                mixed = jnp.dot(mixer, v_n[part], preferred_element_type=f32) + shift
                at = pl.multiple_of(i * step + b * blk, blk)
                gat[q, t, h, pl.ds(at, blk), :] = (u_act[part] * mixed).astype(bf16)
            return carry

        lax.fori_loop(0, 2, loop, 0)

    def middle_rows(h):
        def loop(p, carry):
            here = pl.ds(pl.multiple_of(p * step, step), step)
            left = jnp.concatenate([gat[k % 2, k // 2, h, here, :] for k in range(8)], axis=1)
            value = jnp.dot(left, mg[...], preferred_element_type=f32)
            value += xg[p, t, pl.ds(h * step, step), half(mc, q)].astype(f32)
            mid[q, t, h, here, :] = value.astype(bf16)
            return carry

        lax.fori_loop(0, 2, loop, 0)

    def norm_two(h):
        def loop(i, carry):
            here = pl.ds(pl.multiple_of(i * small, small), small)
            pieces = [mid[k % 2, k // 2, h, here, :].astype(f32) for k in range(8)]
            at = pl.multiple_of(h * 2 * step + i * small, small)
            norm[pl.ds(at, small), :] = scaled(pieces, gain_two)
            return carry

        lax.fori_loop(0, 2 * per_part, loop, 0)

    def up_rows(h):
        def loop(i, carry):
            here = pl.ds(pl.multiple_of((2 * h + i) * step, step), step)
            pre = jnp.dot(norm[here, :], upg[...], preferred_element_type=f32)
            hid[here, :] = jnp.square(jax.nn.relu(pre)).astype(bf16)
            return carry

        lax.fori_loop(0, 2, loop, 0)

    for h in range(chunks):
        gather_rest(0, h)
        norm_one(h)
        if h == 0:
            for w in range(2):
                own_copy(w).wait()
                for o in others:
                    y_arrived(w, o).wait_recv()
        mix_rows(h)
        gather_start(1, h)

    @pl.when(inner)
    def _():
        z_copy(4, facing).start()

    @pl.when(jnp.logical_not(inner))
    def _():
        z_copy(3, facing).start()

    for o in others:
        forward(2, o)

    @pl.when(inner)
    def _():
        forward(3, facing)

    own_copy(2).wait()
    for h in range(chunks):
        gather_pair(1, h)
    for h in range(chunks):
        gather_rest(1, h)
        if h == 0:
            for o in others:
                y_arrived(2, o).wait_recv()
        middle_rows(h)
        gather_start(2, h)
    z_copy(3, pair).start()
    z_copy(4, across).start()
    z_copy(4, pair).start()

    @pl.when(jnp.logical_not(inner))
    def _():
        z_copy(4, facing).start()

    forward(3, across)
    for h in range(chunks):
        gather_pair(2, h)

    @pl.when(jnp.logical_not(inner))
    def _():
        forward(3, facing)

    for h in range(chunks):
        gather_rest(2, h)
        norm_two(h)

    @pl.when(inner)
    def _():
        forward(4, facing)

    forward(3, pair)
    own_copy(3).wait()
    for o in others:
        y_arrived(3, o).wait_recv()
    for h in range(chunks):
        up_rows(h)

    near, far = z // 2, 1 - z // 2
    order = (2 * near + 1 - c, 2 * near + c, 2 * far + 1 - c, 2 * far + c)

    def ready(quarter):
        @pl.when(quarter == z)
        def _():
            own_copy(4).wait()

        @pl.when(quarter != z)
        def _():
            y_arrived(4, quarter).wait_recv()

    def down_part(quarter, h, p):
        start = pl.multiple_of((2 * h + p) * step, step)
        return jnp.dot(
            hid[pl.ds(start, step), :], dng[quarter], preferred_element_type=f32
        )

    def core_copy(n, h, p):
        return remote(
            c_out.at[n, h, p], c_in.at[n, h, p], c_send.at[n, h, p], c_recv.at[n, h, p], to_c
        )

    def pair_copy(n, h):
        return remote(z_out.at[n, h], z_in.at[n, h], r_send.at[n, h], r_recv.at[n, h], to_z)

    def chip_copy(h):
        return remote(x_out.at[h], x_in.at[h], s_send.at[h], s_recv.at[h], to_x)

    def give(n):
        quarter = order[2 * n]
        ready(quarter)
        for i in range(2 * chunks):
            h, p = i % chunks, (1 - q if i < chunks else q)
            c_out[n, h, p] = down_part(quarter, h, p).astype(bf16)
            core_copy(n, h, p).start()

    def keep(n):
        quarter = order[2 * n + 1]
        ready(quarter)
        for i in range(2 * chunks):
            h, p = i % chunks, (1 - q if i < chunks else q)
            core_copy(n, h, p).wait_recv()
            value = down_part(quarter, h, p) + c_in[n, h, p].astype(f32)
            if i < chunks:
                z_out[n, h] = value.astype(bf16)
                pair_copy(n, h).start()
            else:
                c_in[n, h, p] = value.astype(bf16)

    forward(4, across)
    forward(4, pair)
    give(0)

    @pl.when(jnp.logical_not(inner))
    def _():
        forward(4, facing)

    keep(0)
    give(1)
    keep(1)

    far_slot = jnp.where(near == x, 1, 0)
    own_slot = 1 - far_slot

    def send_far(n):
        for h in range(chunks):
            pair_copy(n, h).wait_recv()
            value = c_in[n, h, q].astype(f32) + z_in[n, h].astype(f32)
            x_out[h] = value.astype(bf16)
            chip_copy(h).start()

    @pl.when(far_slot == 0)
    def _():
        send_far(0)
        for h in range(chunks):
            pair_copy(1, h).wait_recv()

    @pl.when(far_slot == 1)
    def _():
        for h in range(chunks):
            pair_copy(0, h).wait_recv()
        send_far(1)

    for h in range(chunks):
        chip_copy(h).wait_recv()
        value = c_in[own_slot, h, q].astype(f32) + z_in[own_slot, h].astype(f32)
        value += x_in[h].astype(f32)
        here = pl.ds(pl.multiple_of(q * step, step), step)
        stream = jnp.concatenate([mid[0, t, h, here, :], mid[1, t, h, here, :]], axis=1)
        out[pl.ds(h * step, step), :] = (value + stream.astype(f32)).astype(bf16)

    for w in range(5):
        for o in others:
            z_copy(w, o).wait_send()
            y_copy(w, o).wait_send()
    for h in range(chunks):
        for a in range(3):
            for n in range(7):
                gather_copy(a, h, n).wait_send()
        for n in range(2):
            for p in range(2):
                core_copy(n, h, p).wait_send()
            pair_copy(n, h).wait_send()
        chip_copy(h).wait_send()


def fused(tokens, first_gain, u_proj, v_proj, group_gain, spatial, spatial_bias, mix_proj,
          second_gain, up_proj, down_proj):
    rows, width = tokens.shape
    both, wide, gw = 2 * rows, second_gain.shape[0], group_gain.shape[1]
    vmem, bf16, dma = pltpu.VMEM, jnp.bfloat16, pltpu.SemaphoreType.DMA
    spec = pl.BlockSpec(memory_space=pltpu.VMEM)
    ff = up_proj.shape[1] // 2
    step = 256
    chunks = rows // step
    return pl.pallas_call(
        functools.partial(fused_kernel, step),
        out_shape=jax.ShapeDtypeStruct(tokens.shape, tokens.dtype),
        in_specs=[spec] * 11,
        out_specs=spec,
        scratch_shapes=[
            vmem((2, 4, rows, width), bf16),
            vmem((wide, 2 * gw), bf16),
            vmem((4 * mix_proj.shape[0], width // 2), bf16),
            vmem((wide, ff), bf16),
            vmem((4, ff, down_proj.shape[1]), bf16),
            vmem((both, wide), bf16),
            vmem((2, 4, chunks, 2 * step, gw), bf16),
            vmem((2, 4, chunks, 2 * step, width // 2), bf16),
            vmem((both, ff), bf16),
            vmem((2, chunks, 2, step, width), bf16),
            vmem((2, chunks, 2, step, width), bf16),
            vmem((2, chunks, step, width), bf16),
            vmem((2, chunks, step, width), bf16),
            vmem((chunks, step, width), bf16),
            vmem((chunks, step, width), bf16),
            dma((5, 4)), dma((5, 4)), dma((5, 4)), dma((5, 4)), dma((6,)),
            dma((3, chunks, 7)), dma((3, chunks, 7)),
            dma((2, chunks, 2)), dma((2, chunks, 2)), dma((2, chunks)), dma((2, chunks)),
            dma((chunks,)), dma((chunks,)),
        ],
        compiler_params=pltpu.CompilerParams(
            collective_id=0, has_side_effects=True, vmem_limit_bytes=64 * 1024 * 1000
        ),
    )(
        tokens, first_gain, u_proj, v_proj, group_gain, spatial, spatial_bias, mix_proj,
        second_gain, up_proj, down_proj,
    )


def layer_part(axes, *args):
    tokens, group_gain, spatial = args[0], args[4], args[5]
    fits = (
        axes["grp"] == 2
        and axes["fs"] == 4
        and axes["tp"] == 4
        and group_gain.shape[0] == 2
        and group_gain.shape[1] % 128 == 0
        and tokens.shape[0] % 256 == 0
        and tokens.shape[1] % 256 == 0
        and tokens.shape[1] == args[10].shape[1]
        and 256 % spatial.shape[1] == 0
    )
    return fused(*args) if fits else per_device(*args)


def solution(mesh):
    return jax.shard_map(
        functools.partial(layer_part, dict(mesh.shape)),
        mesh=mesh,
        in_specs=(
            P(("grp", "fs"), "tp"),
            P(),
            P("fs", "tp"),
            P("fs", "tp"),
            P("tp", None),
            P("tp", None, None),
            P("tp", None),
            P("fs", "tp"),
            P(),
            P("fs", "tp"),
            P("tp", "fs"),
        ),
        out_specs=P(("grp", "fs"), "tp"),
        check_vma=False,
    )
```

time: 214 us -> 188 us (0.88)
  Pallas kernels: 206 us -> 186 us
  local copies, waits for them, and re-layouts: 5.83 us -> 1.87 us
    pallas_call x1, Pallas kernels: 206 us -> 186 us  [fused(): pl.pallas_call(functools.partial(fused_kernel, step), out_shape=jax.Shape...]
    broadcast_in_dim x2 -> x0, local copies, waits for them, and re-layouts: 2.57 us -> none  [the longest x1 1.28 us: fused(): first_gain[None]]
where the time goes in v2:
time: 188 us
  Pallas kernels  186 us (99%)
    pallas_call x1, Pallas kernels, fused(): pl.pallas_call(functools.partial(fused_kernel, step), out_shape=jax.Shape...  186 us

profile of v2, /device:TPU:0, one launch (start us, length us, event | category | flops | bytes accessed | tf_op | source)
XLA Modules:
  0.0 187.8 jit_solution(4209327217759392942)
XLA Ops:
  0.0 185.9 %shard_map.109 = bf16[512,512]{1,0:T(8,128)(2,1)} custom-call(bf16[512,512]{1,0:T(8,128)(2,1)} %tok.1, bf16[2048]{0:T(1024)(128)(2,1)} %gain1.1, bf16[512,256]{1,0:T(8,128)(2,1)} %u_w.1, bf16[512,256]{1,0:T(8,128)(2,1)} %v_w.1, bf16[2,128]{1,0:T(2,128)(2,1)} %ggain.1, bf16[2,128,128]{2,1,0:T(8,128)(2,1)} %spat.1, bf16[2,128]{1,0:T(2,128)(2,1)} %bias.1, ...), custom_call_target="tpu_custom_call" | custom-call | tf_op jit(solution)/shard_map/pallas_call | solution.py:540
  185.9 1.9 copy.13

commit v3 on v2

--- a/solution.py
+++ b/solution.py
@@ -112,7 +112,7 @@
     t_core, t_chip = t + 1 - 2 * c, lax.rem(t + 2, 4)
     to_y, to_z = (1 - y, z, t), (y, z_pair, t)
     to_c, to_x = (y, z, t_core), (y, z, t_chip)
-    others = (lax.rem(z + 2, 4), 3 - z, z_pair)
+    across, facing, pair = others = (lax.rem(z + 2, 4), 3 - z, z_pair)
     rows, width = tok.shape
     step = row_step
     f32, bf16 = jnp.float32, jnp.bfloat16
@@ -124,67 +124,72 @@
         )
     pl.semaphore_wait(barrier, 6)
 
-    gw = ggain.shape[1]
-    ur, mr, mc = u_w.shape[0], mix_w.shape[0], mix_w.shape[1] // 2
-    pr, pc = up_w.shape[0], up_w.shape[1] // 2
-    dr = down_w.shape[0] // 2
+    gw, da = ggain.shape[1], u_w.shape[1]
+    ur, mr, pr, dr = u_w.shape[0], mix_w.shape[0], up_w.shape[0], down_w.shape[0] // 2
 
     def half(size, which):
         return pl.ds(pl.multiple_of(which * size, size), size)
 
-    def take(w, par, which):
-        if w == 0:
-            return u_w.at[slice(None) if which is None else half(ur // 2, which), half(gw, par)]
-        if w == 1:
-            return v_w.at[slice(None) if which is None else half(ur // 2, which), half(gw, par)]
-        if w == 2:
-            return mix_w.at[slice(None) if which is None else half(mr // 2, which), half(mc, par)]
-        if w == 3:
-            return up_w.at[slice(None) if which is None else half(pr // 2, which), half(pc, par)]
+    parts = (1, 1, 1, 2, 2)
+
+    def take(w, par, which, k=0):
+        shard = (u_w, v_w, mix_w, up_w, down_w)[w]
+        if w == 4:
+            if which is None:
+                return shard.at[half(dr, par), :]
+            return shard.at[half(dr // 4, 4 * par + 2 * which + k), :]
+        tall = shard.shape[0]
+        cols = slice(None) if w < 3 else half(shard.shape[1] // 2, par)
         if which is None:
-            return down_w.at[half(dr, par), :]
-        return down_w.at[half(dr // 2, 2 * par + which), :]
-
-    def put(w, source, which):
-        if w < 2:
-            cols = pl.ds(w * gw, gw)
+            return shard.at[:, cols]
+        return shard.at[half(tall // 2 // parts[w], parts[w] * which + k), cols]
+
+    def put(w, source, which, k=0):
+        n = parts[w]
+        if w == 4:
             if which is None:
-                return uvg.at[half(ur, source), cols]
-            return uvg.at[half(ur // 2, 2 * source + which), cols]
-        if w == 2:
-            return mg.at[half(mr, source) if which is None else half(mr // 2, 2 * source + which), :]
-        if w == 3:
-            return upg.at[half(pr, source) if which is None else half(pr // 2, 2 * source + which), :]
+                return dng.at[source]
+            return dng.at[source, half(dr // 2 // n, n * which + k), :]
+        whole, tall = ((uvg, ur), (uvg, ur), (mg, mr), (upg, pr))[w]
+        cols = pl.ds(w * da, da) if w < 2 else slice(None)
         if which is None:
-            return dng.at[source]
-        return dng.at[source, half(dr // 2, which), :]
-
-    def z_copy(w, dest):
+            return whole.at[half(tall, source), cols]
+        return whole.at[half(tall // 2 // n, n * (2 * source + which) + k), cols]
+
+    def z_piece(w, dest, k):
         return remote(
-            take(w, lax.rem(dest, 2), y), put(w, z, y), z_send.at[w, dest], z_recv.at[w, z],
-            (y, dest, t),
+            take(w, lax.rem(dest, 2), y, k), put(w, z, y, k), z_send.at[w, dest, k],
+            z_recv.at[w, z, k], (y, dest, t),
         )
 
-    def z_arrived(w, source):
-        return remote(
-            put(w, source, y), put(w, source, y), z_send.at[w, source], z_recv.at[w, source],
-            (y, source, t),
-        )
-
-    def y_copy(w, source):
-        return remote(
-            put(w, source, y), put(w, source, y), y_send.at[w, source], y_recv.at[w, source], to_y
-        )
+    def z_send_all(w, dest):
+        for k in range(parts[w]):
+            z_piece(w, dest, k).start()
+
+    def y_piece(w, source, k):
+        ref = put(w, source, y, k)
+        return remote(ref, ref, y_send.at[w, source, k], y_recv.at[w, source, k], to_y)
 
     def y_arrived(w, source):
-        return remote(
-            put(w, source, 1 - y), put(w, source, 1 - y), y_send.at[w, source],
-            y_recv.at[w, source], to_y,
-        )
+        for k in range(parts[w]):
+            ref = put(w, source, 1 - y, k)
+            remote(
+                ref, ref, y_send.at[w, source, k], y_recv.at[w, source, k], to_y
+            ).wait_recv()
 
     def forward(w, source):
-        z_arrived(w, source).wait_recv()
-        y_copy(w, source).start()
+        for k in range(parts[w]):
+            ref = put(w, source, y, k)
+            remote(
+                ref, ref, z_send.at[w, source, k], z_recv.at[w, source, k], (y, source, t)
+            ).wait_recv()
+            y_piece(w, source, k).start()
+
+    def pass_on(w):
+        ref = put(w, across, y)
+        remote(
+            ref, ref, z_send.at[w, facing, 0], z_recv.at[w, across, 0], (y, pair, t)
+        ).start()
 
     def own_copy(w):
         return pltpu.make_async_copy(take(w, q, None), put(w, z, None), l_sem.at[w])
@@ -207,11 +212,11 @@
 
     def piece(a, h, p, s):
         if a == 0:
-            return xg.at[p, s, pl.ds(h * step, step), :]
-        return (gat, mid)[a - 1].at[p, s, h]
+            return xg.at[s, pl.ds(h * step, step), :]
+        return gat.at[s, h] if a == 1 else mid.at[p, s, h]
 
     def gather_start(a, h):
-        for n in (0, 1, 2):
+        for n in (1, 2, 0)[: 3 if a == 2 else 2]:
             gather_copy(a, h, n).start()
 
     def gather_pair(a, h):
@@ -222,20 +227,20 @@
     def gather_rest(a, h):
         gather_arrived(a, h, 1).wait_recv()
         gather_copy(a, h, 5).start()
-        gather_arrived(a, h, 3).wait_recv()
-        gather_copy(a, h, 6).start()
-        for n in (2, 4, 5, 6):
+        if a == 2:
+            gather_arrived(a, h, 3).wait_recv()
+            gather_copy(a, h, 6).start()
+        for n in (2, 4, 5, 6) if a == 2 else (2, 5):
             gather_arrived(a, h, n).wait_recv()
 
     chunks = rows // step
     inner = (z + 1) // 2 == 1
-    across, facing, pair = others
-
-    own_tok = pltpu.make_async_copy(tok, xg.at[q, t], l_sem.at[5])
+
+    own_tok = pltpu.make_async_copy(tok, xg.at[t], l_sem.at[5])
     own_tok.start()
-    for w in range(2):
-        for o in others:
-            z_copy(w, o).start()
+    for o in (across, pair):
+        for w in range(2):
+            z_send_all(w, o)
     own_tok.wait()
     for h in range(chunks):
         gather_start(0, h)
@@ -244,22 +249,15 @@
 
     @pl.when(inner)
     def _():
-        z_copy(2, facing).start()
-        z_copy(3, facing).start()
-
-    for h in range(chunks):
-        gather_pair(0, h)
-
-    @pl.when(jnp.logical_not(inner))
-    def _():
-        z_copy(2, facing).start()
-
-    for o in (across, pair):
-        z_copy(2, o).start()
-    z_copy(3, across).start()
+        z_send_all(3, facing)
+
     for w in range(2):
-        for o in others:
-            forward(w, o)
+        forward(w, across)
+        pass_on(w)
+    z_send_all(2, across)
+    z_send_all(2, pair)
+    for w in range(2):
+        forward(w, pair)
 
     def scaled(pieces, gain):
         total = pieces[0].shape[0]
@@ -283,62 +281,53 @@
 
     def norm_one(h):
         def loop(i, carry):
-            p, r = i // per_part, pl.multiple_of(lax.rem(i, per_part) * small, small)
-            pieces = [xg[p, s, pl.ds(h * step + r, small), :].astype(f32) for s in range(4)]
-            at = pl.multiple_of(h * 2 * step + i * small, small)
-            norm[pl.ds(at, small), :] = scaled(pieces, gain_one)
+            here = pl.ds(pl.multiple_of(h * step + i * small, small), small)
+            norm[here, :] = scaled([xg[s, here, :].astype(f32) for s in range(4)], gain_one)
             return carry
 
-        lax.fori_loop(0, 2 * per_part, loop, 0)
+        lax.fori_loop(0, per_part, loop, 0)
 
     blk = spat.shape[1]
     lower = lax.broadcasted_iota(jnp.int32, (blk, blk), 0) >= lax.broadcasted_iota(
         jnp.int32, (blk, blk), 1
     )
-    mixer = jnp.where(lower, spat[q].astype(f32), 0.0).astype(bf16)
     eye = lax.broadcasted_iota(jnp.int32, (blk, blk), 0) == lax.broadcasted_iota(
         jnp.int32, (blk, blk), 1
     )
-    bias_row = jnp.where(q == 0, bias[0:1, :].astype(f32), bias[1:2, :].astype(f32))
-    shift = jnp.sum(jnp.where(eye, bias_row, 0.0), axis=1, keepdims=True)
-    gain_g = jnp.where(q == 0, ggain[0:1, :].astype(f32), ggain[1:2, :].astype(f32))
+    mixers, shifts, gains = [], [], []
+    for g in range(da // gw):
+        mixers.append(jnp.where(lower, spat[g].astype(f32), 0.0).astype(bf16))
+        column = jnp.where(eye, bias[g : g + 1, :].astype(f32), 0.0)
+        shifts.append(jnp.sum(column, axis=1, keepdims=True))
+        gains.append(ggain[g : g + 1, :].astype(f32))
 
     def mix_rows(h):
-        def loop(i, carry):
-            here = pl.ds(pl.multiple_of((2 * h + i) * step, step), step)
-            both = jnp.dot(norm[here, :], uvg[...], preferred_element_type=f32)
-            both = jax.nn.gelu(both)
-            u_act = both[:, :gw].astype(bf16).astype(f32)
-            v_act = both[:, gw:]
+        both = jnp.dot(norm[pl.ds(h * step, step), :], uvg[...], preferred_element_type=f32)
+        both = jax.nn.gelu(both)
+        u_act = both[:, :da].astype(bf16).astype(f32)
+        for g in range(da // gw):
+            cols = slice(g * gw, (g + 1) * gw)
+            v_act = both[:, da + g * gw : da + (g + 1) * gw]
             v_n = (
                 v_act
                 * lax.rsqrt(jnp.mean(v_act * v_act, axis=-1, keepdims=True) + EPS)
-                * gain_g
+                * gains[g]
             ).astype(bf16)
             for b in range(step // blk):
                 part = slice(b * blk, (b + 1) * blk)
-                mixed = jnp.dot(mixer, v_n[part], preferred_element_type=f32) + shift
-                at = pl.multiple_of(i * step + b * blk, blk)
-                gat[q, t, h, pl.ds(at, blk), :] = (u_act[part] * mixed).astype(bf16)
-            return carry
-
-        lax.fori_loop(0, 2, loop, 0)
+                mixed = jnp.dot(mixers[g], v_n[part], preferred_element_type=f32) + shifts[g]
+                gat[t, h, part, cols] = (u_act[part, cols] * mixed).astype(bf16)
 
     def middle_rows(h):
-        def loop(p, carry):
-            here = pl.ds(pl.multiple_of(p * step, step), step)
-            left = jnp.concatenate([gat[k % 2, k // 2, h, here, :] for k in range(8)], axis=1)
-            value = jnp.dot(left, mg[...], preferred_element_type=f32)
-            value += xg[p, t, pl.ds(h * step, step), half(mc, q)].astype(f32)
-            mid[q, t, h, here, :] = value.astype(bf16)
-            return carry
-
-        lax.fori_loop(0, 2, loop, 0)
+        left = jnp.concatenate([gat[k, h] for k in range(4)], axis=1)
+        value = jnp.dot(left, mg[...], preferred_element_type=f32)
+        value += tok[pl.ds(h * step, step), :].astype(f32)
+        mid[q, t, h] = value.astype(bf16)
 
     def norm_two(h):
         def loop(i, carry):
-            here = pl.ds(pl.multiple_of(i * small, small), small)
-            pieces = [mid[k % 2, k // 2, h, here, :].astype(f32) for k in range(8)]
+            p, r = i // per_part, pl.multiple_of(lax.rem(i, per_part) * small, small)
+            pieces = [mid[p, k, h, pl.ds(r, small), :].astype(f32) for k in range(4)]
             at = pl.multiple_of(h * 2 * step + i * small, small)
             norm[pl.ds(at, small), :] = scaled(pieces, gain_two)
             return carry
@@ -357,54 +346,49 @@
     for h in range(chunks):
         gather_rest(0, h)
         norm_one(h)
-        if h == 0:
-            for w in range(2):
-                own_copy(w).wait()
-                for o in others:
-                    y_arrived(w, o).wait_recv()
+    forward(2, across)
+    pass_on(2)
+    z_send_all(3, across)
+    for w in range(2):
+        forward(w, facing)
+    for w in range(2):
+        own_copy(w).wait()
+        for o in others:
+            y_arrived(w, o)
+    for h in range(chunks):
         mix_rows(h)
         gather_start(1, h)
+    forward(2, pair)
+    forward(2, facing)
 
     @pl.when(inner)
     def _():
-        z_copy(4, facing).start()
-
-    @pl.when(jnp.logical_not(inner))
-    def _():
-        z_copy(3, facing).start()
-
-    for o in others:
-        forward(2, o)
-
-    @pl.when(inner)
-    def _():
+        z_send_all(4, facing)
         forward(3, facing)
 
     own_copy(2).wait()
-    for h in range(chunks):
-        gather_pair(1, h)
     for h in range(chunks):
         gather_rest(1, h)
         if h == 0:
             for o in others:
-                y_arrived(2, o).wait_recv()
+                y_arrived(2, o)
         middle_rows(h)
         gather_start(2, h)
-    z_copy(3, pair).start()
-    z_copy(4, across).start()
-    z_copy(4, pair).start()
+    forward(3, across)
+    for h in range(chunks):
+        gather_pair(2, h)
 
     @pl.when(jnp.logical_not(inner))
     def _():
-        z_copy(4, facing).start()
-
-    forward(3, across)
-    for h in range(chunks):
-        gather_pair(2, h)
+        z_send_all(3, facing)
+
+    z_send_all(3, pair)
+    z_send_all(4, across)
+    z_send_all(4, pair)
 
     @pl.when(jnp.logical_not(inner))
     def _():
-        forward(3, facing)
+        z_send_all(4, facing)
 
     for h in range(chunks):
         gather_rest(2, h)
@@ -414,10 +398,15 @@
     def _():
         forward(4, facing)
 
+    @pl.when(jnp.logical_not(inner))
+    def _():
+        forward(3, facing)
+
     forward(3, pair)
+    forward(4, across)
     own_copy(3).wait()
     for o in others:
-        y_arrived(3, o).wait_recv()
+        y_arrived(3, o)
     for h in range(chunks):
         up_rows(h)
 
@@ -431,7 +420,7 @@
 
         @pl.when(quarter != z)
         def _():
-            y_arrived(4, quarter).wait_recv()
+            y_arrived(4, quarter)
 
     def down_part(quarter, h, p):
         start = pl.multiple_of((2 * h + p) * step, step)
@@ -471,7 +460,6 @@
             else:
                 c_in[n, h, p] = value.astype(bf16)
 
-    forward(4, across)
     forward(4, pair)
     give(0)
 
@@ -509,17 +497,16 @@
         chip_copy(h).wait_recv()
         value = c_in[own_slot, h, q].astype(f32) + z_in[own_slot, h].astype(f32)
         value += x_in[h].astype(f32)
-        here = pl.ds(pl.multiple_of(q * step, step), step)
-        stream = jnp.concatenate([mid[0, t, h, here, :], mid[1, t, h, here, :]], axis=1)
-        out[pl.ds(h * step, step), :] = (value + stream.astype(f32)).astype(bf16)
+        out[pl.ds(h * step, step), :] = (value + mid[q, t, h].astype(f32)).astype(bf16)
 
     for w in range(5):
         for o in others:
-            z_copy(w, o).wait_send()
-            y_copy(w, o).wait_send()
+            for k in range(parts[w]):
+                z_piece(w, o, k).wait_send()
+                y_piece(w, o, k).wait_send()
     for h in range(chunks):
         for a in range(3):
-            for n in range(7):
+            for n in range(7) if a == 2 else (1, 2, 5):
                 gather_copy(a, h, n).wait_send()
         for n in range(2):
             for p in range(2):
@@ -531,7 +518,7 @@
 def fused(tokens, first_gain, u_proj, v_proj, group_gain, spatial, spatial_bias, mix_proj,
           second_gain, up_proj, down_proj):
     rows, width = tokens.shape
-    both, wide, gw = 2 * rows, second_gain.shape[0], group_gain.shape[1]
+    both, wide, da = 2 * rows, second_gain.shape[0], u_proj.shape[1]
     vmem, bf16, dma = pltpu.VMEM, jnp.bfloat16, pltpu.SemaphoreType.DMA
     spec = pl.BlockSpec(memory_space=pltpu.VMEM)
     ff = up_proj.shape[1] // 2
@@ -543,14 +530,14 @@
         in_specs=[spec] * 11,
         out_specs=spec,
         scratch_shapes=[
-            vmem((2, 4, rows, width), bf16),
-            vmem((wide, 2 * gw), bf16),
-            vmem((4 * mix_proj.shape[0], width // 2), bf16),
+            vmem((4, rows, width), bf16),
+            vmem((wide, 2 * da), bf16),
+            vmem((4 * mix_proj.shape[0], width), bf16),
             vmem((wide, ff), bf16),
             vmem((4, ff, down_proj.shape[1]), bf16),
             vmem((both, wide), bf16),
-            vmem((2, 4, chunks, 2 * step, gw), bf16),
-            vmem((2, 4, chunks, 2 * step, width // 2), bf16),
+            vmem((4, chunks, step, da), bf16),
+            vmem((2, 4, chunks, step, width), bf16),
             vmem((both, ff), bf16),
             vmem((2, chunks, 2, step, width), bf16),
             vmem((2, chunks, 2, step, width), bf16),
@@ -558,7 +545,7 @@
             vmem((2, chunks, step, width), bf16),
             vmem((chunks, step, width), bf16),
             vmem((chunks, step, width), bf16),
-            dma((5, 4)), dma((5, 4)), dma((5, 4)), dma((5, 4)), dma((6,)),
+            dma((5, 4, 2)), dma((5, 4, 2)), dma((5, 4, 2)), dma((5, 4, 2)), dma((6,)),
             dma((3, chunks, 7)), dma((3, chunks, 7)),
             dma((2, chunks, 2)), dma((2, chunks, 2)), dma((2, chunks)), dma((2, chunks)),
             dma((chunks,)), dma((chunks,)),

time: 188 us -> 170 us (0.904)
  the two profiles are of different devices: /device:TPU:0 before, /device:TPU:16 now
where the time goes in v3:
time: 170 us
  Pallas kernels  168 us (99%)
  local copies, waits for them, and re-layouts  1.87 us (1%)
    pallas_call x1, Pallas kernels, fused(): pl.pallas_call(functools.partial(fused_kernel, step), out_shape=jax.Shape...  168 us

profile of v3, /device:TPU:16, one launch (start us, length us, event | category | flops | bytes accessed | tf_op | source)
XLA Modules:
  0.0 170.2 jit_solution(15668925516913592942)
XLA Ops:
  0.0 168.3 %shard_map.109 = bf16[512,512]{1,0:T(8,128)(2,1)} custom-call(bf16[512,512]{1,0:T(8,128)(2,1)} %tok.1, bf16[2048]{0:T(1024)(128)(2,1)} %gain1.1, bf16[512,256]{1,0:T(8,128)(2,1)} %u_w.1, bf16[512,256]{1,0:T(8,128)(2,1)} %v_w.1, bf16[2,128]{1,0:T(2,128)(2,1)} %ggain.1, bf16[2,128,128]{2,1,0:T(8,128)(2,1)} %spat.1, bf16[2,128]{1,0:T(2,128)(2,1)} %bias.1, ...), custom_call_target="tpu_custom_call" | custom-call | tf_op jit(solution)/shard_map/pallas_call | solution.py:527
  168.3 1.9 %copy.13 = bf16[512,512]{1,0:T(8,128)(2,1)} copy(bf16[512,512]{1,0:T(8,128)(2,1)} %shard_map.109) | data formatting | bytes 1048576
